TPU v7x, 32 devices: a whole 2x2x4 slice. The times are simulated.
32 devices in a mesh: ep: 8 (over z, core), tp: 4 (over y, x).
Axes of the slice: x: 2, y: 2, z: 4, core: 2. Of those that a mesh axis runs over, the one named last changes fastest.
Arguments:
- token_rows: bfloat16 [192, 2048], P('ep', 'tp'), may hold values from -6 to 6
- prior_state: float32 [192, 64, 2048], P('ep', None, 'tp'), may hold values from -4 to 4
- first_gain: bfloat16 [2048], replicated, may hold values from 0.099609375 to 1.8984375
- w_recept: bfloat16 [2048, 2048], P(None, 'tp'), may hold values from -0.125 to 0.125
- w_key: bfloat16 [2048, 2048], P(None, 'tp'), may hold values from -0.125 to 0.125
- w_value: bfloat16 [2048, 2048], P(None, 'tp'), may hold values from -0.125 to 0.125
- decay_down: bfloat16 [2048, 96], P('tp'), may hold values from -0.125 to 0.125
- decay_up: bfloat16 [96, 2048], P(None, 'tp'), may hold values from -0.625 to 0.625
- decay_base: float32 [2048], P('tp'), may hold values from -4 to 3
- iclr_down: bfloat16 [2048, 96], P('tp'), may hold values from -0.125 to 0.125
- iclr_up: bfloat16 [96, 2048], P(None, 'tp'), may hold values from -0.625 to 0.625
- iclr_base: float32 [2048], P('tp'), may hold values from -4 to 4
- key_scale: bfloat16 [2048], P('tp'), may hold values from 0.29882812 to 1.5
- key_mix: bfloat16 [2048], P('tp'), may hold values from 0 to 2
- head_gain: bfloat16 [2048], P('tp'), may hold values from 0.099609375 to 1.8984375
- w_out: bfloat16 [2048, 2048], P(None, 'tp'), may hold values from -0.125 to 0.125
- second_gain: bfloat16 [2048], replicated, may hold values from 0.099609375 to 1.8984375
- routes: int32 [192, 4], P('ep'), may hold values from 0 to 7, all different within a row; in each aligned block of 24 rows (0 to 23, 24 to 47, ...) at most 18 rows name the same one
- route_weights: float32 [192, 4], P('ep'), may hold values from 0.2 to 1
- exp_gate: bfloat16 [8, 2048, 2048], P('ep', None, 'tp'), may hold values from -0.125 to 0.125
- exp_up: bfloat16 [8, 2048, 2048], P('ep', None, 'tp'), may hold values from -0.125 to 0.125
- exp_down: bfloat16 [8, 2048, 2048], P('ep', 'tp'), may hold values from -0.125 to 0.125
- dense_gate: bfloat16 [2048, 512], P(None, 'tp'), may hold values from -0.125 to 0.125
- dense_up: bfloat16 [2048, 512], P(None, 'tp'), may hold values from -0.125 to 0.125
- dense_down: bfloat16 [512, 2048], P('tp'), may hold values from -0.25 to 0.25
- dense_mix: bfloat16 [2048], replicated, may hold values from -0.125 to 0.125
Outputs:
- layer_out: bfloat16 [192, 2048], P('ep', 'tp')
- next_state: float32 [192, 64, 2048], P('ep', None, 'tp')
Inputs may be any that keep to these rules, and one draw needn't show every extreme that they name: `routes`: each row names 4 different experts. Among the rows of one index of ep no expert is named by more than 18 rows, and in every draw some expert is named by exactly 18 of them.
All inputs are finite; a program needn't handle non-finite values.
Results may differ from a plain program's by a relative error of at most 0.018.
Values may be sent and summed in bfloat16 or wider, within the bound.
A program may use at most 64 MiB of HBM per device.

v0:
```python
import jax
import jax.numpy as jnp
from jax import lax
from jax.sharding import PartitionSpec as P

HEAD = 64
norm_eps = 1e-06
head_eps = 0.00064
key_eps = 1e-06


def product(left, right):
    return jnp.dot(left, right, preferred_element_type=jnp.float32)


def scale_rows(values, mean_square, gain):
    return (values * lax.rsqrt(mean_square + norm_eps) * gain.astype(jnp.float32)).astype(
        jnp.bfloat16
    )


def first_norm_rows(token_rows, gain):
    own_width = token_rows.shape[1]
    start = lax.axis_index("tp") * own_width
    gathered = lax.all_gather(token_rows, "tp", axis=1, tiled=True)
    values = gathered.astype(jnp.float32)
    full_rows = scale_rows(values, jnp.mean(values * values, axis=1, keepdims=True), gain)
    own_cols = lax.dynamic_slice_in_dim(full_rows, start, own_width, 1)
    return (full_rows, own_cols)


def second_norm_rows(residual, gain):
    own_width = residual.shape[1]
    start = lax.axis_index("tp") * own_width
    gathered = lax.all_gather(residual, "tp", axis=1, tiled=True)
    values = gathered.astype(jnp.float32)
    full_rows = scale_rows(values, jnp.mean(values * values, axis=1, keepdims=True), gain)
    own_cols = lax.dynamic_slice_in_dim(full_rows, start, own_width, 1)
    return (full_rows, own_cols)


def local(
    token_rows,
    prior_state,
    first_gain,
    w_recept,
    w_key,
    w_value,
    decay_down,
    decay_up,
    decay_base,
    iclr_down,
    iclr_up,
    iclr_base,
    key_scale,
    key_mix,
    head_gain,
    w_out,
    second_gain,
    routes,
    route_weights,
    exp_gate,
    exp_up,
    exp_down,
    dense_gate,
    dense_up,
    dense_down,
    dense_mix,
):
    seq_count, own_width = token_rows.shape
    heads_dev = own_width // HEAD
    first_full, first_own = first_norm_rows(token_rows, first_gain)
    decay_low, rate_low = lax.psum(
        (product(first_own, decay_down), product(first_own, iclr_down)), "tp"
    )
    decay_act = jnp.tanh(decay_low).astype(jnp.bfloat16)
    rate_act = rate_low.astype(jnp.bfloat16)
    recept = product(first_full, w_recept).astype(jnp.bfloat16)
    key_rows = product(first_full, w_key).astype(jnp.bfloat16)
    value_rows = product(first_full, w_value).astype(jnp.bfloat16)
    decay_rate = jnp.exp(
        -jnp.exp(-jax.nn.softplus(-(decay_base + product(decay_act, decay_up))) - 0.5)
    )
    iclr_rate = jax.nn.sigmoid(iclr_base + product(rate_act, iclr_up))
    key_float = key_rows.astype(jnp.float32)
    scaled = (key_float * key_scale.astype(jnp.float32)).reshape(seq_count, heads_dev, HEAD)
    removal = scaled * lax.rsqrt(jnp.sum(scaled * scaled, axis=-1, keepdims=True) + key_eps)
    written = (key_float * (1.0 + (iclr_rate - 1.0) * key_mix.astype(jnp.float32))).reshape(
        seq_count, heads_dev, HEAD
    )
    state_grid = prior_state.reshape(seq_count, HEAD, heads_dev, HEAD)
    recall = jnp.sum(state_grid * removal[:, None], axis=-1)
    scaled_removal = removal * iclr_rate.reshape(seq_count, heads_dev, HEAD)
    value_cols = jnp.transpose(
        value_rows.astype(jnp.float32).reshape(seq_count, heads_dev, HEAD), (0, 2, 1)
    )
    state_grid = (
        state_grid * decay_rate.reshape(seq_count, 1, heads_dev, HEAD)
        - recall[..., None] * scaled_removal[:, None]
        + value_cols[..., None] * written[:, None]
    )
    read = jnp.sum(
        state_grid * recept.astype(jnp.float32).reshape(seq_count, 1, heads_dev, HEAD), axis=-1
    )
    read = jnp.transpose(read, (0, 2, 1))
    centered = read - jnp.mean(read, axis=-1, keepdims=True)
    variance = jnp.mean(centered * centered, axis=-1, keepdims=True)
    head_out = (
        centered
        * lax.rsqrt(variance + head_eps)
        * head_gain.astype(jnp.float32).reshape(heads_dev, HEAD)
    )
    head_out = head_out.reshape(seq_count, own_width).astype(jnp.bfloat16)
    heads_all = lax.all_gather(head_out, "tp", axis=1, tiled=True)
    mixer_out = product(heads_all, w_out).astype(jnp.bfloat16)
    residual = (token_rows.astype(jnp.float32) + mixer_out.astype(jnp.float32)).astype(jnp.bfloat16)
    second_full, second_own = second_norm_rows(residual, second_gain)
    dense_hidden = (
        jax.nn.silu(product(second_full, dense_gate)) * product(second_full, dense_up)
    ).astype(jnp.bfloat16)
    dense_out = lax.psum_scatter(
        product(dense_hidden, dense_down).astype(jnp.bfloat16),
        "tp",
        scatter_dimension=1,
        tiled=True,
    ).astype(jnp.float32)
    mix_gate = jax.nn.sigmoid(product(second_full, dense_mix[:, None])[:, 0])
    group_count = lax.axis_size("ep")
    local_experts = exp_gate.shape[0]
    experts = local_experts * group_count
    top_count = routes.shape[1]
    capacity = max(2, 3 * seq_count * top_count // (2 * experts))
    assign_count = seq_count * top_count
    flat_ids = routes.reshape(assign_count)
    onehot = (flat_ids[:, None] == jnp.arange(experts, dtype=jnp.int32)[None, :]).astype(
        jnp.float32
    )
    earlier = (jnp.arange(assign_count)[:, None] > jnp.arange(assign_count)[None, :]).astype(
        jnp.float32
    )
    before = jnp.dot(earlier, onehot, precision=lax.Precision.HIGHEST)
    ranking = jnp.sum(before * onehot, axis=1).astype(jnp.int32)
    slot_index = flat_ids * capacity + ranking
    slot_total = experts * capacity
    slot_onehot = (jnp.arange(slot_total, dtype=jnp.int32)[:, None] == slot_index[None, :]).astype(
        jnp.bfloat16
    )
    repeated = jnp.repeat(second_full, top_count, axis=0)
    outgoing = product(slot_onehot, repeated).astype(jnp.bfloat16)
    outgoing = outgoing.reshape(group_count, local_experts, capacity, second_full.shape[1])
    arrived = lax.all_to_all(outgoing, "ep", split_axis=0, concat_axis=0, tiled=True)
    gate_act = jnp.einsum("secd,edf->secf", arrived, exp_gate, preferred_element_type=jnp.float32)
    up_act = jnp.einsum("secd,edf->secf", arrived, exp_up, preferred_element_type=jnp.float32)
    hidden = (jax.nn.silu(gate_act) * up_act).astype(jnp.bfloat16)
    partial_value = jnp.einsum(
        "secf,efd->secd", hidden, exp_down, preferred_element_type=jnp.float32
    ).astype(jnp.bfloat16)
    partial_value = lax.optimization_barrier(partial_value)
    summed = lax.psum_scatter(
        partial_value.astype(jnp.float32).astype(jnp.bfloat16),
        "tp",
        scatter_dimension=3,
        tiled=True,
    )
    returned = lax.all_to_all(summed, "ep", split_axis=0, concat_axis=0, tiled=True)
    returned = returned.reshape(slot_total, own_width)
    picked = jnp.take(returned, slot_index, axis=0).astype(jnp.float32)
    weighted = picked * route_weights.reshape(assign_count)[:, None]
    routed = jnp.sum(weighted.reshape(seq_count, top_count, own_width), axis=1)
    layer_out = residual.astype(jnp.float32) + routed + mix_gate[:, None] * dense_out
    return (layer_out.astype(jnp.bfloat16), state_grid.reshape(seq_count, HEAD, own_width))


def solution(mesh):
    in_specs = (
        P("ep", "tp"),
        P("ep", None, "tp"),
        P(),
        P(None, "tp"),
        P(None, "tp"),
        P(None, "tp"),
        P("tp", None),
        P(None, "tp"),
        P("tp"),
        P("tp", None),
        P(None, "tp"),
        P("tp"),
        P("tp"),
        P("tp"),
        P("tp"),
        P(None, "tp"),
        P(),
        P("ep", None),
        P("ep", None),
        P("ep", None, "tp"),
        P("ep", None, "tp"),
        P("ep", "tp", None),
        P(None, "tp"),
        P(None, "tp"),
        P("tp", None),
        P(),
    )
    out_specs = (P("ep", "tp"), P("ep", None, "tp"))
    return jax.shard_map(local, mesh=mesh, in_specs=in_specs, out_specs=out_specs, check_vma=False)
```

profile of v0, /device:TPU:0, one launch (start us, length us, event | category | flops | bytes accessed | tf_op | source)
XLA Modules:
  0.0 181.4 jit_solution(9681087698319180133)
XLA Ops:
  7.2 0.8 convert_element_type.135
  8.1 0.7 convert_element_type.138
  8.7 0.8 reshape.209
  9.5 0.7 convert_element_type.130
  10.2 1.3 convert_element_type.149
  11.5 0.8 copy.47
  12.3 0.1 fusion.33
  12.5 0.6 multiply_add_fusion.1
  13.2 10.0 %all_gather.9 = bf16[24,2048]{1,0:T(8,128)(2,1)S(1)} all-gather(bf16[24,512]{1,0:T(8,128)(2,1)} %param.26), channel_id=1, replica_groups=mesh['ep'=8,'tp'=4] {'tp'}, dimensions={1}, use_global_device_ids=true | all-gather | bytes 122880 | tf_op jit(solution)/shard_map/all_gather | solution.py:25
  23.2 0.1 fusion.49
  23.3 0.1 fusion.51
  23.4 1.0 fusion.62
  24.5 1.0 fusion.64
  25.5 2.0 %fusion.29 = f32[24,512]{1,0:T(8,128)S(1)} fusion(bf16[24,2048]{1,0:T(8,128)(2,1)S(1)} %fusion.51, bf16[2048,512]{1,0:T(8,128)(2,1)} %param.29), kind=kOutput, calls=%fused_computation.30 | convolution fusion | flops 50356224 | bytes 2244608 | tf_op jit(solution)/shard_map/dot_general | solution.py:13
  27.6 2.0 %fusion.30 = f32[24,512]{1,0:T(8,128)S(1)} fusion(bf16[24,2048]{1,0:T(8,128)(2,1)S(1)} %fusion.51, bf16[2048,512]{1,0:T(8,128)(2,1)} %param.31), kind=kOutput, calls=%fused_computation.32 | convolution fusion | flops 50356224 | bytes 2244608 | tf_op jit(solution)/shard_map/dot_general | solution.py:13
  29.7 2.0 %broadcast_multiply_fusion.1 = (f32[24,512]{1,0:T(8,128)S(1)}, f32[24,512]{1,0:T(8,128)S(1)}) fusion(f32[512]{0:T(512)S(1)} %convert_element_type.135, bf16[24,2048]{1,0:T(8,128)(2,1)S(1)} %fusion.51, bf16[2048,512]{1,0:T(8,128)(2,1)} %param.30), kind=kOutput, calls=%fused_computation.81 | convolution fusion | flops 50368512 | bytes 2295808 | tf_op jit(solution)/shard_map/dot_general | solution.py:13
  31.8 0.1 multiply_reduce_fusion.4
  32.1 15.2 %all-reduce = (bf16[24,96]{1,0:T(8,128)(2,1)S(1)}, f32[24,96]{1,0:T(8,128)S(1)}) all-reduce(f32[24,96]{1,0:T(8,128)S(1)} %fusion.62, f32[24,96]{1,0:T(8,128)S(1)} %fusion.64), channel_id=1, replica_groups=mesh['ep'=8,'tp'=4] {'tp'}, use_global_device_ids=true, to_apply=%region_4.5 | all-reduce | flops 4608 | bytes 32256 | tf_op jit(solution)/shard_map/psum | solution.py:73
  47.3 0.8 multiply_multiply_fusion
  48.4 0.2 fusion.60
  48.7 0.5 copy-done.10
  49.2 0.3 copy.44
  49.5 5.6 %reshape.195 = f32[24,64,8,64]{3,2,1,0:T(8,128)} reshape(f32[24,64,512]{2,1,0:T(8,128)} %param.27) | data formatting | bytes 6291456 | tf_op jit(solution)/shard_map/reshape | solution.py:91
  55.1 4.7 %multiply_reduce_fusion.1 = f32[24,64,8]{2,1,0:T(8,128)S(1)} fusion(f32[24,64,8,64]{3,2,1,0:T(8,128)} %reshape.195, f32[24,8,64]{2,1,0:T(8,128)S(1)} %get-tuple-element.5), kind=kLoop, calls=%fused_computation.2 | loop fusion | flops 1560576 | bytes 3244032 | tf_op jit(solution)/shard_map/reduce_sum | solution.py:92
  59.8 5.8 %multiply_reduce_fusion = f32[24,64,8]{2,1,0:T(8,128)S(1)} fusion(f32[24,64,8,64]{3,2,1,0:T(8,128)S(1)} %copy-done.1, f32[24,8,64]{2,1,0:T(8,128)S(1)} %reshape.208, f32[24,8,64]{2,1,0:T(8,128)S(1)} %mul.280, f32[24,64,8]{2,1,0:T(8,128)S(1)} %copy.44, f32[24,8,64]{2,1,0:T(8,128)S(1)} %get-tuple-element.4, f32[24,64,8]{2,1,0:T(8,128)S(1)} %multiply_reduce_fusion.1, ...), kind=kLoop, calls=%fused_computation.1 | loop fusion | flops 5492736 | bytes 3489792 | tf_op jit(solution)/shard_map/reduce_sum | solution.py:102
  65.7 0.1 multiply_reduce_fusion.2
  65.8 0.1 multiply_convert_fusion
  66.0 0.2 copy.46
  66.1 0.1 convert_element_type.141
  66.3 8.4 %all_gather.10 = bf16[24,2048]{1,0:T(8,128)(2,1)S(1)} all-gather(bf16[24,512]{1,0:T(8,128)(2,1)S(1)} %convert_element_type.141), channel_id=1, replica_groups=mesh['ep'=8,'tp'=4] {'tp'}, dimensions={1}, use_global_device_ids=true | all-gather | bytes 122880 | tf_op jit(solution)/shard_map/all_gather | solution.py:114
  74.7 2.0 %fusion.28 = bf16[24,512]{1,0:T(8,128)(2,1)S(1)} fusion(bf16[24,2048]{1,0:T(8,128)(2,1)S(1)} %all_gather.10, bf16[2048,512]{1,0:T(8,128)(2,1)} %param.41, bf16[24,512]{1,0:T(8,128)(2,1)S(1)} %copy-done.12), kind=kOutput, calls=%fused_computation.28 | convolution fusion | flops 50393088 | bytes 2244608 | tf_op jit(solution)/shard_map/dot_general | solution.py:13
  76.6 7.3 %all_gather.11 = bf16[24,2048]{1,0:T(8,128)(2,1)S(1)} all-gather(bf16[24,512]{1,0:T(8,128)(2,1)S(1)} %fusion.28), channel_id=1, replica_groups=mesh['ep'=8,'tp'=4] {'tp'}, dimensions={1}, use_global_device_ids=true | all-gather | bytes 122880 | tf_op jit(solution)/shard_map/all_gather | solution.py:35
  84.0 0.1 fusion.52
  84.2 0.6 copy-done.4
  84.8 0.2 broadcast_in_dim.10
  85.0 0.8 reshape.200
  85.9 1.3 convolution_convert_fusion.1
  87.2 1.1 reshape.201
  88.2 25.8 %all_to_all.10 = bf16[8,1,18,2048]{3,2,1,0:T(8,128)(2,1)S(1)} all-to-all(bf16[8,1,18,2048]{3,2,1,0:T(8,128)(2,1)} %bitcast.112), channel_id=1, replica_groups=mesh['ep'=8,'tp'=4] {'ep'}, dimensions={0} | all-to-all | bytes 1179648 | tf_op jit(solution)/shard_map/all_to_all | solution.py:151
  114.0 0.9 copy-done.3
  114.9 2.9 %fusion.6 = f32[8,1,18,512]{3,2,0,1:T(8,128)} fusion(bf16[1,2048,512]{2,1,0:T(8,128)(2,1)} %param.45, bf16[8,1,18,2048]{3,2,1,0:T(8,128)(2,1)S(1)} %all_to_all.10), kind=kOutput, calls=%fused_computation.13 | convolution fusion | flops 301989888 | bytes 2981888 | tf_op jit(solution)/shard_map/secd,edf->secf/dot_general | solution.py:152
  117.9 3.9 %fusion = bf16[8,1,18,2048]{3,2,0,1:T(8,128)(2,1)} fusion(bf16[1,512,2048]{2,1,0:T(8,128)(2,1)S(1)} %copy-done, bf16[1,2048,512]{2,1,0:T(8,128)(2,1)} %param.46, bf16[8,1,18,2048]{3,2,1,0:T(8,128)(2,1)} %copy-done.3, f32[8,1,18,512]{3,2,0,1:T(8,128)} %fusion.6), kind=kOutput, calls=%fused_computation.6 | convolution fusion | flops 604717056 | bytes 5668864 | tf_op jit(solution)/shard_map/secf,efd->secd/dot_general | solution.py:155
  121.8 0.2 reduce-scatter.5.cloned.1.call-start
  122.1 0.8 fusion.80
  122.9 2.2 %convolution_convert_fusion.2 = bf16[24,2048]{1,0:T(8,128)(2,1)} fusion(bf16[128,2048]{1,0:T(8,128)(2,1)} %param.50, bf16[24,2048]{1,0:T(8,128)(2,1)S(1)} %copy-done.5, bf16[2048,128]{1,0:T(8,128)(2,1)} %param.49, f32[24,128]{1,0:T(8,128)} %fusion.80), kind=kOutput, calls=%fused_computation.7 | convolution fusion | flops 25233408 | bytes 1257472 | tf_op jit(solution)/shard_map/dot_general | solution.py:13
  125.1 0.7 broadcast_multiply_fusion.3
  125.8 0.6 convert_element_type.146
  126.4 0.7 reshape.222
  127.1 0.1 mul.306
  127.2 0.8 copy.53
  128.2 0.7 compare_and_fusion
  128.9 0.1 copy.49
  129.0 0.1 fusion.37
  129.1 5.3 %mul.272 = f32[24,64,8,64]{3,2,1,0:T(8,128)} broadcast(f32[24,64,8]{2,1,0:T(8,128)} %copy-done.2), dimensions={0,1,2} | broadcast | bytes 3194880 | tf_op jit(solution)/shard_map/mul | solution.py:99
  134.4 6.3 %mul.315 = f32[24,64,512]{2,1,0:T(8,128)} reshape(f32[24,64,8,64]{3,2,1,0:T(8,128)} %mul.272) | data formatting | bytes 6291456 | tf_op jit(solution)/shard_map/mul | solution.py:99
  140.7 3.8 %mul.276 = f32[24,64,8,64]{3,2,1,0:T(8,128)} broadcast(f32[24,64,8]{2,1,0:T(8,128)S(1)} %copy.44), dimensions={0,1,2} | broadcast | bytes 3194880 | tf_op jit(solution)/shard_map/mul | solution.py:100
  144.5 6.3 %mul.321 = f32[24,64,512]{2,1,0:T(8,128)} reshape(f32[24,64,8,64]{3,2,1,0:T(8,128)} %mul.276) | data formatting | bytes 6291456 | tf_op jit(solution)/shard_map/mul | solution.py:100
  150.8 7.0 %multiply_add_fusion = f32[24,64,512]{2,1,0:T(8,128)} fusion(f32[24,64,512]{2,1,0:T(8,128)} %mul.321, f32[24,64,512]{2,1,0:T(8,128)} %mul.315, f32[24,64,512]{2,1,0:T(8,128)} %param.27, f32[24,512]{1,0:T(8,128)S(1)} %get-tuple-element.7, f32[24,512]{1,0:T(8,128)S(1)} %copy-done.9, f32[24,512]{1,0:T(8,128)S(1)} %copy-done.11), kind=kLoop, calls=%fused_computation.3 | loop fusion | flops 3932160 | bytes 12730368 | tf_op jit(solution)/shard_map/add | solution.py:98
  157.8 3.4 %all-to-all-start.1 = ((bf16[8,1,18,512]{3,2,1,0:T(8,128)(2,1)}), bf16[8,1,18,512]{3,2,1,0:T(8,128)(2,1)S(1)}, u32[]{:S(2)}, u32[]{:S(2)}) async-start(bf16[8,1,18,512]{3,2,1,0:T(8,128)(2,1)} %bitcast.114), calls=%async_computation.2 | async-start | bytes 393216 | tf_op jit(solution)/shard_map/all_to_all | solution.py:165
  161.2 8.2 %all-to-all-done.1 = bf16[8,1,18,512]{3,2,1,0:T(8,128)(2,1)S(1)} async-done(((bf16[8,1,18,512]{3,2,1,0:T(8,128)(2,1)}), bf16[8,1,18,512]{3,2,1,0:T(8,128)(2,1)S(1)}, u32[]{:S(2)}, u32[]{:S(2)}) %all-to-all-start.1) | async-done | bytes 147488 | tf_op jit(solution)/shard_map/all_to_all | solution.py:165
  169.5 0.8 gather_fusion
  170.3 0.2 multiply_reduce_fusion.3
  170.5 2.6 %reduce-scatter.5.cloned.1.call-done = bf16[24,512]{1,0:T(8,128)(2,1)} async-done(((bf16[24,2048]{1,0:T(8,128)(2,1)}), bf16[24,512]{1,0:T(8,128)(2,1)}) %reduce-scatter.5.cloned.1.call-update) | async-done | bytes 24592 | tf_op jit(solution)/shard_map/reduce_scatter | solution.py:121
  173.1 1.4 add_convert_fusion
  (66 shorter events, 1.7 us)
Async XLA Ops:
  7.2 110.7 %copy-start = (bf16[1,512,2048]{2,1,0:T(8,128)(2,1)S(1)}, bf16[1,512,2048]{2,1,0:T(8,128)(2,1)}, u32[]{:S(2)}) copy-start(bf16[1,512,2048]{2,1,0:T(8,128)(2,1)} %param.47) | copy-start | bytes 6291460
  7.2 150.6 %reduce-scatter.3.cloned.1.call-start = ((), (), s32[]{:S(2)}) async-start(), calls=%async_computation.4 | async-start | bytes 983040 | tf_op jit(solution)/shard_map/reduce_scatter | solution.py:159
  12.5 19.2 %copy-start.18 = (f32[96]{0:T(128)}, f32[96]{0:T(128)S(1)}, u32[]{:S(2)}) copy-start(f32[96]{0:T(128)S(1)} %fusion.33) | copy-start | bytes 1156
  27.5 19.9 %copy-start.13 = (bf16[96,512]{1,0:T(8,128)(2,1)S(1)}, bf16[96,512]{1,0:T(8,128)(2,1)}, u32[]{:S(2)}) copy-start(bf16[96,512]{1,0:T(8,128)(2,1)} %param.36) | copy-start | bytes 294916
  27.5 19.9 %copy-start.15 = (f32[512]{0:T(512)S(1)}, f32[512]{0:T(512)}, u32[]{:S(2)}) copy-start(f32[512]{0:T(512)} %param.37) | copy-start | bytes 6148
  27.6 20.8 %copy-start.16 = (bf16[96,512]{1,0:T(8,128)(2,1)S(1)}, bf16[96,512]{1,0:T(8,128)(2,1)}, u32[]{:S(2)}) copy-start(bf16[96,512]{1,0:T(8,128)(2,1)} %param.33) | copy-start | bytes 294916
  27.6 20.8 %copy-start.17 = (f32[512]{0:T(512)S(1)}, f32[512]{0:T(512)}, u32[]{:S(2)}) copy-start(f32[512]{0:T(512)} %param.34) | copy-start | bytes 6148
  48.6 0.6 copy-start.10
  55.1 4.7 %copy-start.1 = (f32[24,64,8,64]{3,2,1,0:T(8,128)S(1)}, f32[24,64,8,64]{3,2,1,0:T(8,128)}, u32[]{:S(2)}) copy-start(f32[24,64,8,64]{3,2,1,0:T(8,128)} %reshape.195) | copy-start | bytes 9437188
  59.8 5.8 %copy-start.2 = (f32[24,64,8]{2,1,0:T(8,128)}, f32[24,64,8]{2,1,0:T(8,128)S(1)}, u32[]{:S(2)}) copy-start(f32[24,64,8]{2,1,0:T(8,128)S(1)} %multiply_reduce_fusion.1) | copy-start | bytes 147460
  65.6 9.1 %copy-start.12 = (bf16[24,512]{1,0:T(8,128)(2,1)S(1)}, bf16[24,512]{1,0:T(8,128)(2,1)}, u32[]{:S(2)}) copy-start(bf16[24,512]{1,0:T(8,128)(2,1)} %param.26) | copy-start | bytes 73732
  65.6 18.5 %copy-start.14 = (f32[2048]{0:T(1024)S(1)}, f32[2048]{0:T(1024)}, u32[]{:S(2)}) copy-start(f32[2048]{0:T(1024)} %convert_element_type.149) | copy-start | bytes 24580
  76.6 7.5 %copy-start.7 = (bf16[24,512]{1,0:T(8,128)(2,1)}, bf16[24,512]{1,0:T(8,128)(2,1)S(1)}, u32[]{:S(2)}) copy-start(bf16[24,512]{1,0:T(8,128)(2,1)S(1)} %fusion.28) | copy-start | bytes 73732
  84.2 0.6 copy-start.4
  114.0 0.9 copy-start.3
  117.9 4.2 %copy-start.5 = (bf16[24,2048]{1,0:T(8,128)(2,1)S(1)}, bf16[24,2048]{1,0:T(8,128)(2,1)}, u32[]{:S(2)}) copy-start(bf16[24,2048]{1,0:T(8,128)(2,1)} %copy-done.4) | copy-start | bytes 294916
  117.9 4.2 %copy-start.6 = (bf16[2048,128]{1,0:T(8,128)(2,1)S(1)}, bf16[2048,128]{1,0:T(8,128)(2,1)}, u32[]{:S(2)}) copy-start(bf16[2048,128]{1,0:T(8,128)(2,1)} %param.48) | copy-start | bytes 1572868
  121.8 51.3 %reduce-scatter.5.cloned.1.call-start = ((), (), s32[]{:S(2)}) async-start(), calls=%async_computation.5 | async-start | bytes 122880 | tf_op jit(solution)/shard_map/reduce_scatter | solution.py:121
  144.5 6.3 %copy-start.9 = (f32[24,512]{1,0:T(8,128)S(1)}, f32[24,512]{1,0:T(8,128)}, u32[]{:S(2)}) copy-start(f32[24,512]{1,0:T(8,128)} %get-tuple-element.6) | copy-start | bytes 147460
  144.5 6.3 %copy-start.11 = (f32[24,512]{1,0:T(8,128)S(1)}, f32[24,512]{1,0:T(8,128)}, u32[]{:S(2)}) copy-start(f32[24,512]{1,0:T(8,128)} %copy-done.10) | copy-start | bytes 147460
  150.8 10.4 %copy-start.19 = (f32[96]{0:T(128)S(1)}, f32[96]{0:T(128)}, u32[]{:S(2)}) copy-start(f32[96]{0:T(128)} %copy-done.18) | copy-start | bytes 1156
  150.8 22.3 %copy-start.8 = (bf16[24,512]{1,0:T(8,128)(2,1)S(1)}, bf16[24,512]{1,0:T(8,128)(2,1)}, u32[]{:S(2)}) copy-start(bf16[24,512]{1,0:T(8,128)(2,1)} %copy-done.7) | copy-start | bytes 73732
  157.8 11.6 %all-to-all-start.1 = ((bf16[8,1,18,512]{3,2,1,0:T(8,128)(2,1)}), bf16[8,1,18,512]{3,2,1,0:T(8,128)(2,1)S(1)}, u32[]{:S(2)}, u32[]{:S(2)}) async-start(bf16[8,1,18,512]{3,2,1,0:T(8,128)(2,1)} %bitcast.114), calls=%async_computation.2 | async-start | bytes 393216 | tf_op jit(solution)/shard_map/all_to_all | solution.py:165
Sparse Core Ops, SparseCore 0:
  121.9 24.2 reduce-scatter.2
  149.0 24.0 reduce-scatter.4
where the time goes:
time: 183 us; the launch traced here: 181 us
  blocking collectives  66.8 us (37%)
  local copies, waits for them, and re-layouts  37.1 us (20%)
  other arithmetic  26.2 us (14%)
  matrix products  22.4 us (12%)
  between operations  14.4 us (8%)
  waiting for transfers between devices  10.8 us (6%)
  starting transfers between devices  3.65 us (2%)
    all_to_all x1, blocking collectives, local(): lax.all_to_all(outgoing, 'ep', split_axis=0, concat_axis=0, tiled=True)  25.8 us
    dot_general x12, matrix products, product(): return jnp.dot(left, right, preferred_element_type=jnp.float32)  15.4 us
    psum x1, blocking collectives, local(): lax.psum((product(first_own, decay_down), product(first_own, iclr_down)),...  15.2 us
    mul x2, local copies, waits for them, and re-layouts, local(): recall[..., None] * scaled_removal[:, None]  11.6 us
    mul x3, local copies, waits for them, and re-layouts, local(): value_cols[..., None] * written[:, None]  10.1 us
    all_gather x1, blocking collectives, first_norm_rows(): gathered = lax.all_gather(token_rows, 'tp', axis=1, tiled=True)  10 us
    all_gather x1, blocking collectives, local(): heads_all = lax.all_gather(head_out, 'tp', axis=1, tiled=True)  8.39 us
    all_to_all x1, waiting for transfers between devices, local(): lax.all_to_all(summed, 'ep', split_axis=0, concat_axis=0, tiled=True)  8.19 us
  transfers between devices with their start and end apart: 3, of which 2 were waited for; matrix products, arithmetic and copies ran while one was open for 20% of the time, Pallas kernels for 0%

commit v1 on v0

--- a/solution.py
+++ b/solution.py
@@ -22,7 +22,12 @@
 def first_norm_rows(token_rows, gain):
     own_width = token_rows.shape[1]
     start = lax.axis_index("tp") * own_width
-    gathered = lax.all_gather(token_rows, "tp", axis=1, tiled=True)
+    ring = [token_rows]
+    for hop in range(3):
+        ring.append(lax.ppermute(ring[-1], "tp", [(dev, (dev + 1) % 4) for dev in range(4)]))
+    gathered = jnp.roll(
+        jnp.concatenate(ring[::-1], axis=1), (lax.axis_index("tp") + 1) * ring[0].shape[1], axis=1
+    )
     values = gathered.astype(jnp.float32)
     full_rows = scale_rows(values, jnp.mean(values * values, axis=1, keepdims=True), gain)
     own_cols = lax.dynamic_slice_in_dim(full_rows, start, own_width, 1)

time: 183 us -> 184 us (level)
  blocking collectives: 66.8 us -> 33.2 us
  waiting for transfers between devices: 10.8 us -> 40.7 us
  starting transfers between devices: 3.65 us -> 13.6 us
  matrix products: 22.4 us -> 19.3 us
    all_to_all x1 -> x0, blocking collectives: 25.8 us -> none  [local(): lax.all_to_all(outgoing, 'ep', split_axis=0, concat_axis=0, tiled=True)]
    all_to_all x0 -> x1, waiting for transfers between devices: none -> 21 us  [local(): lax.all_to_all(outgoing, 'ep', split_axis=0, concat_axis=0, tiled=True)]
    reduce_scatter x1, waiting for transfers between devices: 2.57 us -> 12.9 us  [local(): lax.psum_scatter(product(dense_hidden, dense_down).astype(jnp.bfloat16),...]
    all_gather x1 -> x0, blocking collectives: 10 us -> none  [first_norm_rows(): gathered = lax.all_gather(token_rows, 'tp', axis=1, tiled=True)]
    all_to_all x1, waiting for transfers between devices: 8.19 us -> 1.14 us  [local(): lax.all_to_all(summed, 'ep', split_axis=0, concat_axis=0, tiled=True)]
    ppermute x0 -> x3, waiting for transfers between devices: none -> 5.64 us  [first_norm_rows(): lax.ppermute(ring[-1], 'tp', [(dev, (dev + 1) % 4) for dev in range(4)])]
    all_to_all x0 -> x1, starting transfers between devices: none -> 4.88 us  [local(): lax.all_to_all(outgoing, 'ep', split_axis=0, concat_axis=0, tiled=True)]
    ppermute x0 -> x3, starting transfers between devices: none -> 4.33 us  [first_norm_rows(): lax.ppermute(ring[-1], 'tp', [(dev, (dev + 1) % 4) for dev in range(4)])]
  transfers between devices with their start and end apart: 3 -> 7, of which waited for: 2 -> 5; matrix products, arithmetic and copies ran while one was open for 20% -> 24% of each run, Pallas kernels for 0% -> 0%
where the time goes in v1:
time: 184 us; the launch traced here: 183 us
  waiting for transfers between devices  40.7 us (22%)
  local copies, waits for them, and re-layouts  35.5 us (19%)
  blocking collectives  33.2 us (18%)
  other arithmetic  26 us (14%)
  matrix products  19.3 us (10%)
  between operations  14.6 us (8%)
  starting transfers between devices  13.6 us (7%)
    all_to_all x1, waiting for transfers between devices, local(): lax.all_to_all(outgoing, 'ep', split_axis=0, concat_axis=0, tiled=True)  21 us
    psum x1, blocking collectives, local(): lax.psum((product(first_own, decay_down), product(first_own, iclr_down)),...  17.1 us
    reduce_scatter x1, waiting for transfers between devices, local(): lax.psum_scatter(product(dense_hidden, dense_down).astype(jnp.bfloat16),...  12.9 us
    dot_general x12, matrix products, product(): return jnp.dot(left, right, preferred_element_type=jnp.float32)  12.9 us
    mul x2, local copies, waits for them, and re-layouts, local(): recall[..., None] * scaled_removal[:, None]  11.4 us
    mul x3, local copies, waits for them, and re-layouts, local(): value_cols[..., None] * written[:, None]  10.2 us
    reduce_sum x1, other arithmetic, local(): jnp.sum(state_grid * recept.astype(jnp.float32).reshape(seq_count, 1, hea...  8.51 us
    all_gather x1, blocking collectives, local(): heads_all = lax.all_gather(head_out, 'tp', axis=1, tiled=True)  8.26 us
  transfers between devices with their start and end apart: 7, of which 5 were waited for; matrix products, arithmetic and copies ran while one was open for 24% of the time, Pallas kernels for 0%

profile of v1, /device:TPU:0, one launch (start us, length us, event | category | flops | bytes accessed | tf_op | source)
XLA Modules:
  0.0 182.7 jit_solution(7930463979639800963)
XLA Ops:
  7.2 3.0 %collective-permute-start = (bf16[24,512]{1,0:T(8,128)(2,1)}, bf16[24,512]{1,0:T(8,128)(2,1)S(1)}, u32[]{:S(2)}, u32[]{:S(2)}) collective-permute-start(bf16[24,512]{1,0:T(8,128)(2,1)} %param.26), channel_id=1, source_target_pairs={{0,1},{1,2},{2,3},{3,0},{4,5},{5,6},{6,7},{7,4},{8,9},{9,10},{10,1... | collective-permute-start | bytes 73736 | tf_op jit(solution)/shard_map/ppermute | solution.py:27
  10.2 0.8 copy.47
  11.0 0.1 reshape.199
  11.1 2.1 %collective-permute-done = bf16[24,512]{1,0:T(8,128)(2,1)S(1)} collective-permute-done((bf16[24,512]{1,0:T(8,128)(2,1)}, bf16[24,512]{1,0:T(8,128)(2,1)S(1)}, u32[]{:S(2)}, u32[]{:S(2)}) %collective-permute-start) | collective-permute-done | bytes 24608 | tf_op jit(solution)/shard_map/ppermute | solution.py:27
  13.2 1.1 collective-permute-start.1
  14.2 0.1 fusion.33
  14.4 3.5 %collective-permute-done.1 = bf16[24,512]{1,0:T(8,128)(2,1)S(1)} collective-permute-done((bf16[24,512]{1,0:T(8,128)(2,1)S(1)}, bf16[24,512]{1,0:T(8,128)(2,1)S(1)}, u32[]{:S(2)}, u32[]{:S(2)}) %collective-permute-start.1) | collective-permute-done | bytes 24608 | tf_op jit(solution)/shard_map/ppermute | solution.py:27
  17.9 0.2 collective-permute-start.2
  18.1 0.5 multiply_add_fusion.1
  18.7 0.7 convert_element_type.135
  19.4 0.7 convert_element_type.138
  20.1 0.8 reshape.209
  20.8 0.7 convert_element_type.130
  21.5 0.7 convert_element_type.149
  22.2 0.7 copy.45
  22.9 5.6 %reshape.195 = f32[24,64,8,64]{3,2,1,0:T(8,128)} reshape(f32[24,64,512]{2,1,0:T(8,128)} %param.27) | data formatting | bytes 6291456 | tf_op jit(solution)/shard_map/reshape | solution.py:96
  28.6 0.1 fusion.49
  28.9 0.1 fusion.62
  29.0 0.1 fusion.64
  29.2 2.0 %fusion.29 = f32[24,512]{1,0:T(8,128)S(1)} fusion(bf16[24,2048]{1,0:T(8,128)(2,1)S(1)} %fusion.51, bf16[2048,512]{1,0:T(8,128)(2,1)} %param.29), kind=kOutput, calls=%fused_computation.30 | convolution fusion | flops 50356224 | bytes 2244608 | tf_op jit(solution)/shard_map/dot_general | solution.py:13
  31.3 2.0 %fusion.30 = f32[24,512]{1,0:T(8,128)S(1)} fusion(bf16[24,2048]{1,0:T(8,128)(2,1)S(1)} %fusion.51, bf16[2048,512]{1,0:T(8,128)(2,1)} %param.31), kind=kOutput, calls=%fused_computation.32 | convolution fusion | flops 50356224 | bytes 2244608 | tf_op jit(solution)/shard_map/dot_general | solution.py:13
  33.4 2.0 %broadcast_multiply_fusion.1 = (f32[24,512]{1,0:T(8,128)S(1)}, f32[24,512]{1,0:T(8,128)S(1)}) fusion(f32[512]{0:T(512)S(1)} %convert_element_type.135, bf16[24,2048]{1,0:T(8,128)(2,1)S(1)} %fusion.51, bf16[2048,512]{1,0:T(8,128)(2,1)} %param.30), kind=kOutput, calls=%fused_computation.81 | convolution fusion | flops 50368512 | bytes 2295808 | tf_op jit(solution)/shard_map/dot_general | solution.py:13
  35.3 0.1 reshape.196
  35.4 0.1 multiply_reduce_fusion.4
  35.7 17.1 %all-reduce = (bf16[24,96]{1,0:T(8,128)(2,1)S(1)}, f32[24,96]{1,0:T(8,128)S(1)}) all-reduce(f32[24,96]{1,0:T(8,128)S(1)} %fusion.62, f32[24,96]{1,0:T(8,128)S(1)} %fusion.64), channel_id=1, replica_groups=mesh['ep'=8,'tp'=4] {'tp'}, use_global_device_ids=true, to_apply=%region_4.5 | all-reduce | flops 4608 | bytes 32256 | tf_op jit(solution)/shard_map/psum | solution.py:78
  52.8 0.8 multiply_multiply_fusion
  53.9 0.2 fusion.60
  54.1 0.5 copy-done.10
  54.7 0.3 copy.44
  55.0 4.5 %multiply_reduce_fusion.1 = f32[24,64,8]{2,1,0:T(8,128)S(1)} fusion(f32[24,64,8,64]{3,2,1,0:T(8,128)} %reshape.195, f32[24,8,64]{2,1,0:T(8,128)S(1)} %get-tuple-element.5), kind=kLoop, calls=%fused_computation.2 | loop fusion | flops 1560576 | bytes 3244032 | tf_op jit(solution)/shard_map/reduce_sum | solution.py:97
  59.5 8.5 %multiply_reduce_fusion = f32[24,64,8]{2,1,0:T(8,128)S(1)} fusion(f32[24,64,8,64]{3,2,1,0:T(8,128)} %reshape.195, f32[24,8,64]{2,1,0:T(8,128)S(1)} %reshape.208, f32[24,8,64]{2,1,0:T(8,128)S(1)} %mul.284, f32[24,64,8]{2,1,0:T(8,128)S(1)} %copy.44, f32[24,8,64]{2,1,0:T(8,128)S(1)} %get-tuple-element.4, f32[24,64,8]{2,1,0:T(8,128)S(1)} %multiply_reduce_fusion.1, ...), kind=kLoop, calls=%fused_computation.1 | loop fusion | flops 5492736 | bytes 3489792 | tf_op jit(solution)/shard_map/reduce_sum | solution.py:107
  68.1 0.1 multiply_reduce_fusion.2
  68.3 0.1 multiply_convert_fusion
  68.4 0.2 copy.46
  68.6 0.1 convert_element_type.141
  68.7 8.3 %all_gather.6 = bf16[24,2048]{1,0:T(8,128)(2,1)S(1)} all-gather(bf16[24,512]{1,0:T(8,128)(2,1)S(1)} %convert_element_type.141), channel_id=1, replica_groups=mesh['ep'=8,'tp'=4] {'tp'}, dimensions={1}, use_global_device_ids=true | all-gather | bytes 122880 | tf_op jit(solution)/shard_map/all_gather | solution.py:119
  77.0 2.0 %fusion.28 = bf16[24,512]{1,0:T(8,128)(2,1)S(1)} fusion(bf16[24,2048]{1,0:T(8,128)(2,1)S(1)} %all_gather.6, bf16[2048,512]{1,0:T(8,128)(2,1)} %param.41, bf16[24,512]{1,0:T(8,128)(2,1)S(1)} %copy-done.6), kind=kOutput, calls=%fused_computation.28 | convolution fusion | flops 50393088 | bytes 2244608 | tf_op jit(solution)/shard_map/dot_general | solution.py:13
  79.0 7.8 %all_gather.7 = bf16[24,2048]{1,0:T(8,128)(2,1)S(1)} all-gather(bf16[24,512]{1,0:T(8,128)(2,1)S(1)} %fusion.28), channel_id=1, replica_groups=mesh['ep'=8,'tp'=4] {'tp'}, dimensions={1}, use_global_device_ids=true | all-gather | bytes 122880 | tf_op jit(solution)/shard_map/all_gather | solution.py:40
  86.8 0.1 fusion.52
  87.1 0.6 copy-done.2
  87.7 0.2 broadcast_in_dim.10
  87.9 0.8 reshape.200
  88.7 1.3 convolution_convert_fusion.1
  90.0 1.1 reshape.201
  91.1 4.9 %all-to-all-start = ((bf16[8,1,18,2048]{3,2,1,0:T(8,128)(2,1)}), bf16[8,1,18,2048]{3,2,1,0:T(8,128)(2,1)}, u32[]{:S(2)}, u32[]{:S(2)}) async-start(bf16[8,1,18,2048]{3,2,1,0:T(8,128)(2,1)} %bitcast.112), calls=%async_computation | async-start | bytes 1572864 | tf_op jit(solution)/shard_map/all_to_all | solution.py:156
  96.1 21.0 %all-to-all-done = bf16[8,1,18,2048]{3,2,1,0:T(8,128)(2,1)} async-done(((bf16[8,1,18,2048]{3,2,1,0:T(8,128)(2,1)}), bf16[8,1,18,2048]{3,2,1,0:T(8,128)(2,1)}, u32[]{:S(2)}, u32[]{:S(2)}) %all-to-all-start) | async-done | bytes 589856 | tf_op jit(solution)/shard_map/all_to_all | solution.py:156
  117.0 2.4 %fusion.6 = f32[8,1,18,512]{3,2,0,1:T(8,128)S(1)} fusion(bf16[1,2048,512]{2,1,0:T(8,128)(2,1)} %param.45, bf16[8,1,18,2048]{3,2,1,0:T(8,128)(2,1)} %all-to-all-done), kind=kOutput, calls=%fused_computation.13 | convolution fusion | flops 301989888 | bytes 2981888 | tf_op jit(solution)/shard_map/secd,edf->secf/dot_general | solution.py:157
  119.5 3.8 %fusion = bf16[8,1,18,2048]{3,2,0,1:T(8,128)(2,1)} fusion(bf16[1,512,2048]{2,1,0:T(8,128)(2,1)S(1)} %copy-done, bf16[1,2048,512]{2,1,0:T(8,128)(2,1)} %param.46, bf16[8,1,18,2048]{3,2,1,0:T(8,128)(2,1)} %all-to-all-done, f32[8,1,18,512]{3,2,0,1:T(8,128)S(1)} %fusion.6), kind=kOutput, calls=%fused_computation.6 | convolution fusion | flops 604717056 | bytes 5668864 | tf_op jit(solution)/shard_map/secf,efd->secd/dot_general | solution.py:160
  123.5 0.1 mul.310
  123.9 0.1 copy.49
  124.0 5.1 %mul.276 = f32[24,64,8,64]{3,2,1,0:T(8,128)} broadcast(f32[24,64,8]{2,1,0:T(8,128)} %copy-done.1), dimensions={0,1,2} | broadcast | bytes 3194880 | tf_op jit(solution)/shard_map/mul | solution.py:104
  129.1 6.3 %mul.319 = f32[24,64,512]{2,1,0:T(8,128)} reshape(f32[24,64,8,64]{3,2,1,0:T(8,128)} %mul.276) | data formatting | bytes 6291456 | tf_op jit(solution)/shard_map/mul | solution.py:104
  135.4 3.8 %mul.280 = f32[24,64,8,64]{3,2,1,0:T(8,128)} broadcast(f32[24,64,8]{2,1,0:T(8,128)S(1)} %copy.44), dimensions={0,1,2} | broadcast | bytes 3194880 | tf_op jit(solution)/shard_map/mul | solution.py:105
  139.2 6.4 %mul.325 = f32[24,64,512]{2,1,0:T(8,128)} reshape(f32[24,64,8,64]{3,2,1,0:T(8,128)} %mul.280) | data formatting | bytes 6291456 | tf_op jit(solution)/shard_map/mul | solution.py:105
  145.6 0.2 fusion.80
  145.8 2.0 %convolution_convert_fusion.2 = bf16[24,2048]{1,0:T(8,128)(2,1)} fusion(bf16[128,2048]{1,0:T(8,128)(2,1)S(1)} %copy-done.5, bf16[24,2048]{1,0:T(8,128)(2,1)S(1)} %copy-done.3, bf16[2048,128]{1,0:T(8,128)(2,1)} %param.49, f32[24,128]{1,0:T(8,128)S(1)} %fusion.80), kind=kOutput, calls=%fused_computation.7 | convolution fusion | flops 25233408 | bytes 1257472 | tf_op jit(solution)/shard_map/dot_general | solution.py:13
  147.9 4.3 %all-to-all-start.1 = ((bf16[8,1,18,512]{3,2,1,0:T(8,128)(2,1)}), bf16[8,1,18,512]{3,2,1,0:T(8,128)(2,1)S(1)}, u32[]{:S(2)}, u32[]{:S(2)}) async-start(bf16[8,1,18,512]{3,2,1,0:T(8,128)(2,1)} %bitcast.114), calls=%async_computation.2 | async-start | bytes 393216 | tf_op jit(solution)/shard_map/all_to_all | solution.py:170
  152.2 7.0 %multiply_add_fusion = f32[24,64,512]{2,1,0:T(8,128)} fusion(f32[24,64,512]{2,1,0:T(8,128)} %mul.325, f32[24,64,512]{2,1,0:T(8,128)} %mul.319, f32[24,64,512]{2,1,0:T(8,128)} %param.27, f32[24,512]{1,0:T(8,128)S(1)} %get-tuple-element.7, f32[24,512]{1,0:T(8,128)S(1)} %copy-done.9, f32[24,512]{1,0:T(8,128)S(1)} %copy-done.11), kind=kLoop, calls=%fused_computation.3 | loop fusion | flops 3932160 | bytes 12730368 | tf_op jit(solution)/shard_map/add | solution.py:103
  159.2 0.1 fusion.37
  159.4 1.1 all-to-all-done.1
  160.6 0.8 gather_fusion
  161.4 0.2 multiply_reduce_fusion.3
  161.6 12.9 %reduce-scatter.5.cloned.1.call-done = bf16[24,512]{1,0:T(8,128)(2,1)} async-done(((bf16[24,2048]{1,0:T(8,128)(2,1)}), bf16[24,512]{1,0:T(8,128)(2,1)}) %reduce-scatter.5.cloned.1.call-update) | async-done | bytes 24592 | tf_op jit(solution)/shard_map/reduce_scatter | solution.py:126
  174.5 1.4 add_convert_fusion
  (88 shorter events, 1.7 us)
Async XLA Ops:
  7.2 112.3 %copy-start = (bf16[1,512,2048]{2,1,0:T(8,128)(2,1)S(1)}, bf16[1,512,2048]{2,1,0:T(8,128)(2,1)}, u32[]{:S(2)}) copy-start(bf16[1,512,2048]{2,1,0:T(8,128)(2,1)} %param.47) | copy-start | bytes 6291460
  7.2 6.0 %collective-permute-start = (bf16[24,512]{1,0:T(8,128)(2,1)}, bf16[24,512]{1,0:T(8,128)(2,1)S(1)}, u32[]{:S(2)}, u32[]{:S(2)}) collective-permute-start(bf16[24,512]{1,0:T(8,128)(2,1)} %param.26), channel_id=1, source_target_pairs={{0,1},{1,2},{2,3},{3,0},{4,5},{5,6},{6,7},{7,4},{8,9},{9,10},{10,1... | collective-permute-start | bytes 73736 | tf_op jit(solution)/shard_map/ppermute | solution.py:27
  13.2 4.7 %collective-permute-start.1 = (bf16[24,512]{1,0:T(8,128)(2,1)S(1)}, bf16[24,512]{1,0:T(8,128)(2,1)S(1)}, u32[]{:S(2)}, u32[]{:S(2)}) collective-permute-start(bf16[24,512]{1,0:T(8,128)(2,1)S(1)} %collective-permute-done), channel_id=1, source_target_pairs={{0,1},{1,2},{2,3},{3,0},{4,5},{5,6},{6,7},{7,4},{8,9},{9,10},{10,1... | collective-permute-start | bytes 73736 | tf_op jit(solution)/shard_map/ppermute | solution.py:27
  14.4 4.3 %copy-start.22 = (f32[96]{0:T(128)}, f32[96]{0:T(128)S(1)}, u32[]{:S(2)}) copy-start(f32[96]{0:T(128)S(1)} %fusion.33) | copy-start | bytes 1156
  17.9 10.6 %collective-permute-start.2 = (bf16[24,512]{1,0:T(8,128)(2,1)S(1)}, bf16[24,512]{1,0:T(8,128)(2,1)S(1)}, u32[]{:S(2)}, u32[]{:S(2)}) collective-permute-start(bf16[24,512]{1,0:T(8,128)(2,1)S(1)} %collective-permute-done.1), channel_id=1, source_target_pairs={{0,1},{1,2},{2,3},{3,0},{4,5},{5,6},{6,7},{7,4},{8,9},{9,10},{10,1... | collective-permute-start | bytes 73736 | tf_op jit(solution)/shard_map/ppermute | solution.py:27
  22.9 5.7 %copy-start.6 = (bf16[24,512]{1,0:T(8,128)(2,1)S(1)}, bf16[24,512]{1,0:T(8,128)(2,1)}, u32[]{:S(2)}) copy-start(bf16[24,512]{1,0:T(8,128)(2,1)} %param.26) | copy-start | bytes 73732
  22.9 6.0 %copy-start.13 = (bf16[512,96]{0,1:T(8,128)(2,1)S(1)}, bf16[512,96]{0,1:T(8,128)(2,1)}, u32[]{:S(2)}) copy-start(bf16[512,96]{0,1:T(8,128)(2,1)} %param.35) | copy-start | bytes 294916
  22.9 6.1 %copy-start.14 = (bf16[512,96]{0,1:T(8,128)(2,1)S(1)}, bf16[512,96]{0,1:T(8,128)(2,1)}, u32[]{:S(2)}) copy-start(bf16[512,96]{0,1:T(8,128)(2,1)} %param.32) | copy-start | bytes 294916
  31.1 21.7 %copy-start.15 = (bf16[96,512]{1,0:T(8,128)(2,1)S(1)}, bf16[96,512]{1,0:T(8,128)(2,1)}, u32[]{:S(2)}) copy-start(bf16[96,512]{1,0:T(8,128)(2,1)} %param.36) | copy-start | bytes 294916
  31.1 21.7 %copy-start.18 = (f32[512]{0:T(512)S(1)}, f32[512]{0:T(512)}, u32[]{:S(2)}) copy-start(f32[512]{0:T(512)} %param.37) | copy-start | bytes 6148
  31.2 22.6 %copy-start.20 = (bf16[96,512]{1,0:T(8,128)(2,1)S(1)}, bf16[96,512]{1,0:T(8,128)(2,1)}, u32[]{:S(2)}) copy-start(bf16[96,512]{1,0:T(8,128)(2,1)} %param.33) | copy-start | bytes 294916
  31.3 22.6 %copy-start.21 = (f32[512]{0:T(512)S(1)}, f32[512]{0:T(512)}, u32[]{:S(2)}) copy-start(f32[512]{0:T(512)} %param.34) | copy-start | bytes 6148
  54.1 0.6 copy-start.10
  59.5 8.5 %copy-start.1 = (f32[24,64,8]{2,1,0:T(8,128)}, f32[24,64,8]{2,1,0:T(8,128)S(1)}, u32[]{:S(2)}) copy-start(f32[24,64,8]{2,1,0:T(8,128)S(1)} %multiply_reduce_fusion.1) | copy-start | bytes 147460
  59.5 8.8 %copy-start.12 = (f32[8,64]{0,1:T(8,128)S(1)}, f32[8,64]{0,1:T(8,128)}, u32[]{:S(2)}) copy-start(f32[8,64]{0,1:T(8,128)} %copy.45) | copy-start | bytes 6148
  79.0 8.0 %copy-start.7 = (bf16[24,512]{1,0:T(8,128)(2,1)}, bf16[24,512]{1,0:T(8,128)(2,1)S(1)}, u32[]{:S(2)}) copy-start(bf16[24,512]{1,0:T(8,128)(2,1)S(1)} %fusion.28) | copy-start | bytes 73732
  79.0 17.0 %copy-start.23 = (f32[96]{0:T(128)S(1)}, f32[96]{0:T(128)}, u32[]{:S(2)}) copy-start(f32[96]{0:T(128)} %copy-done.22) | copy-start | bytes 1156
  79.0 17.1 %copy-start.17 = (bf16[2048]{0:T(1024)(128)(2,1)S(1)}, bf16[2048]{0:T(1024)(128)(2,1)}, u32[]{:S(2)}) copy-start(bf16[2048]{0:T(1024)(128)(2,1)} %param.51) | copy-start | bytes 12292
  87.1 0.6 copy-start.2
  91.1 25.9 %all-to-all-start = ((bf16[8,1,18,2048]{3,2,1,0:T(8,128)(2,1)}), bf16[8,1,18,2048]{3,2,1,0:T(8,128)(2,1)}, u32[]{:S(2)}, u32[]{:S(2)}) async-start(bf16[8,1,18,2048]{3,2,1,0:T(8,128)(2,1)} %bitcast.112), calls=%async_computation | async-start | bytes 1572864 | tf_op jit(solution)/shard_map/all_to_all | solution.py:156
  96.0 51.9 %reduce-scatter.3.cloned.1.call-start = ((), (), s32[]{:S(2)}) async-start(), calls=%async_computation.4 | async-start | bytes 983040 | tf_op jit(solution)/shard_map/reduce_scatter | solution.py:164
  119.5 3.9 %copy-start.16 = (s32[24,4]{0,1:T(4,128)S(1)}, s32[24,4]{0,1:T(4,128)}, u32[]{:S(2)}) copy-start(s32[24,4]{0,1:T(4,128)} %param.43) | copy-start | bytes 1156
  119.5 4.1 %copy-start.19 = (f32[24,4]{0,1:T(4,128)S(1)}, f32[24,4]{0,1:T(4,128)}, u32[]{:S(2)}) copy-start(f32[24,4]{0,1:T(4,128)} %param.44) | copy-start | bytes 1156
  123.3 51.1 %reduce-scatter.5.cloned.1.call-start = ((), (), s32[]{:S(2)}) async-start(), calls=%async_computation.5 | async-start | bytes 122880 | tf_op jit(solution)/shard_map/reduce_scatter | solution.py:126
  139.2 6.4 %copy-start.3 = (bf16[24,2048]{1,0:T(8,128)(2,1)S(1)}, bf16[24,2048]{1,0:T(8,128)(2,1)}, u32[]{:S(2)}) copy-start(bf16[24,2048]{1,0:T(8,128)(2,1)} %copy-done.2) | copy-start | bytes 294916
  139.2 6.4 %copy-start.4 = (bf16[2048,128]{1,0:T(8,128)(2,1)S(1)}, bf16[2048,128]{1,0:T(8,128)(2,1)}, u32[]{:S(2)}) copy-start(bf16[2048,128]{1,0:T(8,128)(2,1)} %param.48) | copy-start | bytes 1572868
  139.2 6.6 %copy-start.5 = (bf16[128,2048]{1,0:T(8,128)(2,1)S(1)}, bf16[128,2048]{1,0:T(8,128)(2,1)}, u32[]{:S(2)}) copy-start(bf16[128,2048]{1,0:T(8,128)(2,1)} %param.50) | copy-start | bytes 1572868
  139.2 13.0 %copy-start.9 = (f32[24,512]{1,0:T(8,128)S(1)}, f32[24,512]{1,0:T(8,128)}, u32[]{:S(2)}) copy-start(f32[24,512]{1,0:T(8,128)} %get-tuple-element.6) | copy-start | bytes 147460
  139.2 13.0 %copy-start.11 = (f32[24,512]{1,0:T(8,128)S(1)}, f32[24,512]{1,0:T(8,128)}, u32[]{:S(2)}) copy-start(f32[24,512]{1,0:T(8,128)} %copy-done.10) | copy-start | bytes 147460
  147.9 12.6 %all-to-all-start.1 = ((bf16[8,1,18,512]{3,2,1,0:T(8,128)(2,1)}), bf16[8,1,18,512]{3,2,1,0:T(8,128)(2,1)S(1)}, u32[]{:S(2)}, u32[]{:S(2)}) async-start(bf16[8,1,18,512]{3,2,1,0:T(8,128)(2,1)} %bitcast.114), calls=%async_computation.2 | async-start | bytes 393216 | tf_op jit(solution)/shard_map/all_to_all | solution.py:170
  152.2 22.3 %copy-start.8 = (bf16[24,512]{1,0:T(8,128)(2,1)S(1)}, bf16[24,512]{1,0:T(8,128)(2,1)}, u32[]{:S(2)}) copy-start(bf16[24,512]{1,0:T(8,128)(2,1)} %copy-done.7) | copy-start | bytes 73732
Sparse Core Ops, SparseCore 0:
  123.5 24.0 reduce-scatter.2
  150.3 24.0 reduce-scatter.4
